TPU v7x, 256 devices: a whole 4x4x8 slice. The times are simulated.
256 devices in a mesh: sp: 32 (over z, x), tp: 4 (over y), dp: 2 (over core).
Axes of the slice: x: 4, y: 4, z: 8, core: 2. Of those that a mesh axis runs over, the one named last changes fastest.
Arguments:
- latent: bfloat16 [2, 6144, 2048], P('dp', 'sp'), may hold values from -6 to 6
- cond: bfloat16 [2, 2048], P('dp', 'sp'), may hold values from -6 to 6
- context: bfloat16 [2, 256, 2048], P('dp', 'sp'), may hold values from -6 to 6
- ctx_cond: bfloat16 [2048], P('sp'), may hold values from -6 to 6
- w_mod: bfloat16 [2048, 6144], P('sp', 'tp'), may hold values from -0.125 to 0.125
- norm_gain: bfloat16 [2048], replicated, may hold values from 0.099609375 to 1.8984375
- w_query: bfloat16 [2048, 1024], P(None, 'tp'), may hold values from -0.125 to 0.125
- w_key: bfloat16 [2048, 1024], P(None, 'tp'), may hold values from -0.125 to 0.125
- w_value: bfloat16 [2048, 1024], P(None, 'tp'), may hold values from -0.125 to 0.125
- w_outgate: bfloat16 [2048, 1024], P(None, 'tp'), may hold values from -0.125 to 0.125
- w_decay: bfloat16 [2048, 2, 8], P(None, None, 'tp'), may hold values from -0.125 to 0.125
- w_beta: bfloat16 [2048, 2, 8], P(None, None, 'tp'), may hold values from -0.125 to 0.125
- decay_rate: float32 [2, 8], P(None, 'tp'), may hold values from 8.138021e-06 to 0.0333333333
- decay_bias: float32 [2, 8], P(None, 'tp'), may hold values from -3 to 3
- extra_decay: float32 [2, 2, 8, 6144], P('dp', None, 'tp', 'sp'), may hold values from -0.7000977 to -1.6276042e-05
- out_gain: bfloat16 [128], replicated, may hold values from 0.099609375 to 1.8984375
- w_out: bfloat16 [1024, 2048], replicated, may hold values from -0.1875 to 0.1875
Outputs:
- mixed_out: bfloat16 [2, 6144, 2048], P('dp', ('sp', 'tp'))
All inputs are finite; a program needn't handle non-finite values.
Results may differ from a plain program's by a relative error of at most 0.0067.
Values may be sent and summed in bfloat16 or wider, within the bound.
A program may use at most 128 MiB of HBM per device.

v0:
```python
import functools

import jax
import jax.numpy as jnp
from jax import lax
from jax.experimental import pallas as pl
from jax.experimental.pallas import tpu as pltpu
from jax.sharding import Mesh
from jax.sharding import PartitionSpec as P

D = 2048
HEAD = 128
BLOCK = 64
HEADS_DEV = 2
CHAINS = 2 * HEADS_DEV
HALF = HEAD // 2
MAP_ROWS = HEAD + HALF + 16
ZAX, XAX, YAX = "sp_0", "sp_1", "tp"
SP = (ZAX, XAX)
SP_TP = (ZAX, XAX, YAX)
MESH = pl.DeviceIdType.MESH
F32 = jnp.float32
BF16 = jnp.bfloat16

norm_eps = 1e-06
beta_scale = 30.0

NN = (((1,), (0,)), ((), ()))
NT = (((1,), (1,)), ((), ()))
TN = (((0,), (0,)), ((), ()))


def dot16(left, right, dims=NN):
    return lax.dot_general(left, right, dims, preferred_element_type=F32)


def mm1(left, right, dims=NN):
    return dot16(left.astype(BF16), right.astype(BF16), dims)


def halves(values):
    high = values.astype(BF16)
    return high, (values - high.astype(F32)).astype(BF16)


def mm3(left, right, dims=NN):
    left_high, left_low = halves(left)
    right_high, right_low = halves(right)
    return dot16(left_high, right_high, dims) + (
        dot16(left_high, right_low, dims) + dot16(left_low, right_high, dims)
    )


def mm_exact_left(left, right, dims=NN):
    high, low = halves(right)
    left = left.astype(BF16)
    return dot16(left, high, dims) + dot16(left, low, dims)


def mm_full(left, right, dims=NN):
    return lax.dot_general(
        left, right, dims, preferred_element_type=F32, precision=lax.Precision.HIGHEST
    )


def silu(values):
    return values * jax.nn.sigmoid(values)


def softplus(values):
    return jnp.maximum(values, 0.0) + jnp.log1p(jnp.exp(-jnp.abs(values)))


def unit_normal(values):
    return values * lax.rsqrt(jnp.sum(values * values, axis=-1, keepdims=True) + norm_eps)


def iota2(shape, dim):
    return lax.broadcasted_iota(jnp.int32, shape, dim)


def unit_inverses(lows, places):
    eye = (iota2((BLOCK, BLOCK), 0) == iota2((BLOCK, BLOCK), 1)).astype(F32)

    def coupling(low, place, level):
        row, col = place
        joined = (row >> (level + 1)) == (col >> (level + 1))
        mask = joined & (((row >> level) & 1) == 1) & (((col >> level) & 1) == 0)
        return jnp.where(mask, low, 0.0)

    results = [eye - coupling(low, place, 0) for low, place in zip(lows, places)]
    for level in range(1, (BLOCK - 1).bit_length()):
        inner = [
            mm3(coupling(low, place, level), result)
            for low, place, result in zip(lows, places, results)
        ]
        results = [result - mm3(result, term) for result, term in zip(results, inner)]
    return results


def chain_terms(keys, values, gram, sums, final, betas, place):
    row, col = place
    eye = iota2((BLOCK, BLOCK), 0) == iota2((BLOCK, BLOCK), 1)
    wide = jnp.broadcast_to(sums, (BLOCK, BLOCK))
    across = jnp.sum(jnp.where(eye, wide, 0.0), axis=0, keepdims=True)
    lower = row >= col
    weights = jnp.where(lower, jnp.exp(jnp.where(lower, wide - across, 0.0)), 0.0)
    low = jnp.where(row > col, gram * betas * weights, 0.0)
    grown = jnp.exp(sums)
    scaled = keys * betas
    right = jnp.concatenate([scaled * grown, values * betas], axis=1)
    decayed = keys * jnp.exp(final - sums)
    return low, right, decayed, weights, grown


def round16(values):
    return values.astype(BF16).astype(F32)


def pack_halves(values):
    return jnp.concatenate([values[: HEAD // 2], values[HEAD // 2 :]], axis=1)


def unpack_halves(values):
    return jnp.concatenate([values[:, : HEAD // 2], values[:, HEAD // 2 :]], axis=0)


def decay_rows(decay):
    high = round16(decay)
    middle = round16(decay - high)
    last = decay - high - middle
    row = iota2((16, HEAD), 0)
    pieces = jnp.where(row == 0, high, jnp.where(row == 1, middle, last))
    return jnp.where(row < 3, pieces, 0.0).astype(BF16)


def put_map(ref, index, decay, near, offset):
    ref[index, :HEAD, :] = near.astype(BF16)
    ref[index, HEAD : HEAD + HALF, :] = pack_halves(offset).astype(BF16)
    ref[index, HEAD + HALF :, :] = decay_rows(decay)


def get_map(ref, index):
    pieces = ref[index, HEAD + HALF :, :].astype(F32)
    decay = pieces[0:1] + pieces[1:2] + pieces[2:3]
    offset = unpack_halves(ref[index, HEAD : HEAD + HALF, :].astype(F32))
    return decay, ref[index, :HEAD, :], offset


def context_steps(ctx_all, rate, bias, direction, h, half):
    nx, nz, rows, _ = ctx_all.shape
    tokens = nx * nz * rows
    data = jnp.concatenate(
        [ctx_all[i, j].astype(F32) for j in range(nz) for i in range(nx)], axis=0
    )
    keys_all = unit_normal(silu(data[:, :HEAD]))
    values_all = silu(
        jnp.where(half == 0, data[:, HEAD : HEAD + HALF], data[:, HEAD + HALF : 2 * HEAD])
    )
    rates = data[:, 2 * HEAD :]
    lane = iota2(rates.shape, 1)
    mine = direction * HEADS_DEV + h
    decay_raw = jnp.sum(jnp.where(lane == mine, rates, 0.0), axis=1, keepdims=True)
    beta_raw = jnp.sum(jnp.where(lane == mine + CHAINS, rates, 0.0), axis=1, keepdims=True)
    log_decay = -rate * softplus(decay_raw + bias)
    betas = jax.nn.sigmoid(beta_raw) * (beta_scale * rate)
    row, col = iota2((BLOCK, BLOCK), 0), iota2((BLOCK, BLOCK), 1)
    flip = direction * (BLOCK - 1)
    sign = 1 - 2 * direction
    place = (flip + sign * row, flip + sign * col)
    tri = (place[0] >= place[1]).astype(F32)
    jobs, lows = [], []
    for b in range(tokens // BLOCK):
        part = slice(b * BLOCK, (b + 1) * BLOCK)
        sums = mm_full(tri, jnp.broadcast_to(log_decay[part], (BLOCK, HEAD)))[:, :1]
        final = jnp.sum(log_decay[part], axis=0, keepdims=True)
        keys, values = keys_all[part], values_all[part]
        gram = mm3(keys, keys, NT)
        low, right, decayed, _, _ = chain_terms(
            keys, values, gram, sums, final, betas[part], place
        )
        lows.append(low)
        jobs.append((right, decayed, final))
    steps = []
    for (right, decayed, final), inverse in zip(jobs, unit_inverses(lows, [place] * len(lows))):
        steps.append((mm1(decayed, mm3(inverse, right), TN), jnp.exp(final)))
    return steps


LOADED = [
    "cond",
    "ctx_cond",
    "w_mod",
    "latent",
    "context",
    "gain",
    "w_key",
    "w_value",
    "w_decay",
    "w_beta",
    "extra",
    "w_query",
    "w_outgate",
    "out_gain",
    "w_out",
    "rate",
    "bias",
]
IN_SMEM = ("rate", "bias")
COMM = ["mod1", "mod2", "ctx", "ctx2", "near", "far", "back", "tp"]


def whole_kernel(nz, nx, ny, hbm, out_ref, loads, load_sem, mem, send, recv):
    z, x, y = lax.axis_index(ZAX), lax.axis_index(XAX), lax.axis_index(YAX)
    span = loads["latent"].shape[1]
    ctx_rows = loads["context"].shape[1]
    blocks = span // BLOCK
    rows_out = span // ny
    inner = HEADS_DEV * HEAD
    low_z = lax.rem(z, 2)
    group = z // 2
    groups = nz // 2
    members = 2 * nx
    own_head, own_half, direction = x // 2, lax.rem(x, 2), low_z
    sign = 1 - 2 * direction

    across = [(dx, dy) for dx in range(nx) for dy in range(ny) if (dx, dy) != (0, 0)]
    across.sort(key=lambda at: -min(at[0], nx - at[0]) - min(at[1], ny - at[1]))
    close = [(dl, dx) for dl in range(2) for dx in range(nx) if (dl, dx) != (0, 0)]
    close.sort(key=lambda at: -at[0] - min(at[1], nx - at[1]))
    along = sorted(range(1, nz), key=lambda dz: -min(dz, nz - dz))

    def across_target(dx, dy):
        return {XAX: lax.rem(x + dx, nx), YAX: lax.rem(y + dy, ny)}

    def close_place(dl, dx):
        return lax.rem(low_z + dl, 2), lax.rem(x + dx, nx)

    barrier = pltpu.get_barrier_semaphore()
    peers = [{ZAX: lax.rem(z + dz, nz)} for dz in range(1, nz)]
    peers += [across_target(*at) for at in across]
    peers += [
        {ZAX: group * 2 + lax.rem(low_z + 1, 2), XAX: lax.rem(x + dx, nx)} for dx in range(1, nx)
    ]
    for target in peers:
        pl.semaphore_signal(barrier, inc=1, device_id=target, device_id_type=MESH)
    fetched = {}
    rate_ref, bias_ref = loads["rate"], loads["bias"]
    for i, name in enumerate(LOADED):
        fetched[name] = pltpu.make_async_copy(hbm[name], loads[name], load_sem.at[i])
        fetched[name].start()

    def remote(kind, k, source, destination, target):
        return pltpu.make_async_remote_copy(
            src_ref=source,
            dst_ref=destination,
            send_sem=send[kind].at[k],
            recv_sem=recv[kind].at[k],
            device_id=target,
            device_id_type=MESH,
        )

    started = []

    def begin(copy):
        copy.start()
        started.append(copy)
        return copy

    part, slots, spread = mem["part"], mem["mod_slots"], mem["spread"]
    width = part.shape[1]
    for name in ("cond", "ctx_cond", "w_mod"):
        fetched[name].wait()
    cond = jnp.concatenate(
        [loads["cond"][...].astype(F32), loads["ctx_cond"][...].astype(F32)], axis=0
    )
    part[...] = dot16(silu(cond).astype(BF16), loads["w_mod"][...])
    pl.semaphore_wait(barrier, len(peers))
    arriving = [
        begin(remote("mod1", dz, part, slots.at[dz], {ZAX: lax.rem(z + dz, nz)})) for dz in along
    ]
    for name in ("latent", "context", "gain"):
        fetched[name].wait()
    gain = jnp.concatenate(
        [loads["gain"][i : i + 1, :].astype(F32) for i in range(D // HEAD)], axis=1
    )

    def normed(values):
        values = values.astype(F32)
        mean = jnp.mean(values * values, axis=-1, keepdims=True)
        return values * lax.rsqrt(mean + norm_eps) * gain

    mem["normed"][:span, :] = normed(loads["latent"][0])
    mem["normed"][span : span + ctx_rows, :] = normed(loads["context"][0])

    summed = part[...]
    for dz, copy in reversed(list(zip(along, arriving))):
        copy.wait_recv()
        summed = summed + slots[dz]
    spread[y * nx + x] = summed
    arriving = [
        begin(
            remote(
                "mod2",
                dy * nx + dx,
                spread.at[y * nx + x],
                spread.at[y * nx + x],
                across_target(dx, dy),
            )
        )
        for dx, dy in across
    ]
    for name in ("w_key", "w_value", "w_decay", "w_beta", "extra", "rate", "bias"):
        fetched[name].wait()
    small = jnp.concatenate(
        [loads[name][d].astype(F32) for name in ("w_decay", "w_beta") for d in range(2)], axis=0
    ).astype(BF16)
    extra = jnp.concatenate([loads["extra"][0, d] for d in range(2)], axis=0)
    eye_span = (iota2((span, span), 0) == iota2((span, span), 1)).astype(F32)
    added = mm_full(eye_span, extra, NT)
    for copy in arriving:
        copy.wait_recv()
    mod = mem["mod"]
    for j in range(ny):
        summed = spread[j * nx]
        for i in range(1, nx):
            summed = summed + spread[j * nx + i]
        mod[:, j * width : (j + 1) * width] = summed

    rows = mem["rows"]
    rows[:span, :] = (
        mem["normed"][:span, :] * (1.0 + mod[0:1, D : 2 * D]) + mod[0:1, :D]
    ).astype(BF16)
    ctx_in = mem["normed"][span : span + ctx_rows, :] * (1.0 + mod[1:2, D : 2 * D]) + mod[1:2, :D]
    rows[span:, :] = jnp.concatenate(
        [ctx_in, jnp.zeros((rows.shape[0] - span - ctx_rows, D), F32)], axis=0
    ).astype(BF16)
    key_raw = round16(dot16(rows[...], loads["w_key"][...]))
    value_raw = round16(dot16(rows[...], loads["w_value"][...]))
    rates_raw = round16(dot16(rows[...], small, NT))

    ctx_z, ctx_all = mem["ctx_z"], mem["ctx_all"]
    ctx_rates = jnp.concatenate(
        [rates_raw[span : span + ctx_rows], jnp.zeros((ctx_rows, HEAD - 2 * CHAINS), F32)], axis=1
    )
    for h in range(HEADS_DEV):
        lanes = slice(h * HEAD, (h + 1) * HEAD)
        ctx_z[h, z] = jnp.concatenate(
            [
                key_raw[span : span + ctx_rows, lanes],
                value_raw[span : span + ctx_rows, lanes],
                ctx_rates,
            ],
            axis=1,
        ).astype(BF16)
    ctx_arriving = [
        begin(
            remote(
                "ctx",
                h * nz + dz,
                ctx_z.at[h, z],
                ctx_z.at[h, z],
                {ZAX: lax.rem(z + dz, nz)},
            )
        )
        for dz in along
        for h in range(HEADS_DEV)
    ]

    lane4 = iota2((1, CHAINS), 1)

    def by_lane(ref):
        line = jnp.zeros((1, CHAINS), F32)
        for d in range(2):
            for h in range(HEADS_DEV):
                line = jnp.where(lane4 == d * HEADS_DEV + h, ref[d, h], line)
        return line

    rate = by_lane(rate_ref)
    log_decay = -rate * softplus(rates_raw[:span, :CHAINS] + by_lane(bias_ref)) + added
    betas = jax.nn.sigmoid(rates_raw[:span, CHAINS:]) * (beta_scale * rate)
    row, col = iota2((BLOCK, BLOCK), 0), iota2((BLOCK, BLOCK), 1)
    places = [(row, col), (BLOCK - 1 - row, BLOCK - 1 - col)]
    tris = [(row >= col).astype(F32), (row <= col).astype(F32)]
    sums = [
        [mm_full(tris[d], log_decay[b * BLOCK : (b + 1) * BLOCK]) for b in range(blocks)]
        for d in range(2)
    ]
    jobs, lows, orders, key_parts = [], [], [], {}
    for h in range(HEADS_DEV):
        lanes = slice(h * HEAD, (h + 1) * HEAD)
        keys_h = unit_normal(silu(key_raw[:span, lanes]))
        values_h = silu(value_raw[:span, lanes])
        for b in range(blocks):
            at = slice(b * BLOCK, (b + 1) * BLOCK)
            keys, values = keys_h[at], values_h[at]
            key_parts[h, b] = keys
            gram = mm3(keys, keys, NT)
            for d in range(2):
                lane = d * HEADS_DEV + h
                cums = sums[d][b][:, lane : lane + 1]
                final = cums[BLOCK - 1 : BLOCK] if d == 0 else cums[0:1]
                low, right, decayed, weights, grown = chain_terms(
                    keys, values, gram, cums, final, betas[at, lane : lane + 1], places[d]
                )
                lows.append(low)
                orders.append(places[d])
                jobs.append((h, d, b, right, decayed, weights, grown, final))
    inverses = unit_inverses(lows, orders)
    found = {}
    for (h, d, b, right, decayed, weights, grown, final), inverse in zip(jobs, inverses):
        solved = mm3(inverse, right)
        step = mm1(decayed, solved, TN)
        found[h, d, b] = (-step[:, :HEAD], step[:, HEAD:], jnp.exp(final), solved, weights, grown)
    maps = mem["maps"]
    before = {}
    for h in range(HEADS_DEV):
        for d in range(2):
            whole = None
            for b in range(blocks) if d == 0 else reversed(range(blocks)):
                near, offset, decay = found[h, d, b][:3]
                before[h, d, b] = whole
                if whole is None:
                    whole = (decay, near, offset)
                else:
                    decay_all, near_all, offset_all = whole
                    moved = mm1(near, jnp.concatenate([near_all, offset_all], axis=1))
                    whole = (
                        decay * decay_all,
                        decay * near_all + decay_all * near + moved[:, :HEAD],
                        decay * offset_all + moved[:, HEAD:] + offset,
                    )
            decay, near, offset = whole
            for c in range(2):
                index = (2 * h + d) * 2 + c
                put_map(maps, index, decay, near, offset[:, c * HALF : (c + 1) * HALF])

    near_slots = mem["near_slots"]

    def map_index(low, at_x):
        return ((at_x // 2) * 2 + low) * 2 + lax.rem(at_x, 2)

    near_slots[0] = maps[map_index(low_z, x)]
    arriving = []
    for dl, dx in close:
        low, at_x = close_place(dl, dx)
        arriving.append(
            begin(
                remote(
                    "near",
                    dl * nx + dx,
                    maps.at[map_index(low, at_x)],
                    near_slots.at[dl * nx + dx],
                    {ZAX: group * 2 + low, XAX: at_x},
                )
            )
        )

    for copy in ctx_arriving:
        copy.wait_recv()
    ctx_all[x] = ctx_z[own_head]
    ctx_arriving = []
    for dx in range(1, nx):
        to = lax.rem(x + dx, nx)
        ctx_arriving.append(
            begin(remote("ctx2", dx, ctx_z.at[to // 2], ctx_all.at[x], {XAX: to}))
        )

    for name in ("w_query", "w_outgate", "out_gain"):
        fetched[name].wait()
    query_raw = round16(dot16(rows[:span, :], loads["w_query"][...]))
    mem["gate"][...] = silu(round16(dot16(rows[:span, :], loads["w_outgate"][...])))
    reads, base = mem["reads"], mem["base"]
    for h in range(HEADS_DEV):
        lanes = slice(h * HEAD, (h + 1) * HEAD)
        queries_h = unit_normal(silu(query_raw[:, lanes])) * HEAD ** (-0.5)
        for b in range(blocks):
            at = slice(b * BLOCK, (b + 1) * BLOCK)
            queries = queries_h[at]
            cross = mm1(queries, key_parts[h, b], NT)
            fixed = None
            for d in range(2):
                _, _, _, solved, weights, grown = found[h, d, b]
                read = mm1(cross * weights, solved)
                reader = queries * grown - read[:, :HEAD]
                now = read[:, HEAD:]
                to = slice(d * HEAD, (d + 1) * HEAD)
                if before[h, d, b] is None:
                    reads[h, at, to] = reader.astype(BF16)
                else:
                    decay_all, near_all, offset_all = before[h, d, b]
                    moved = mm1(reader, jnp.concatenate([near_all, offset_all], axis=1))
                    reads[h, at, to] = (decay_all * reader + moved[:, :HEAD]).astype(BF16)
                    now = now + moved[:, HEAD:]
                fixed = now if fixed is None else fixed + now
            base[h, at, :] = fixed

    for copy in arriving:
        copy.wait_recv()
    prefix_near, prefix_offset, prefix_decay = (
        mem["prefix_near"],
        mem["prefix_offset"],
        mem["prefix_decay"],
    )
    whole = None
    for p in range(members):
        source = p + direction * (members - 1 - 2 * p)
        from_low, from_x = source // nx, lax.rem(source, nx)
        slot = lax.rem(low_z - from_low + 2, 2) * nx + lax.rem(x - from_x + nx, nx)
        decay, near16, offset = get_map(near_slots, slot)
        near = near16.astype(F32)
        if whole is None:
            prefix_near[0] = jnp.zeros((HEAD, HEAD), BF16)
            prefix_offset[0] = jnp.zeros((HEAD, HALF), F32)
            prefix_decay[0] = jnp.ones((8, HALF), F32)
            whole = (decay, near, offset)
        else:
            decay_all, near_all, offset_all = whole
            prefix_near[p] = near_all.astype(BF16)
            prefix_offset[p] = offset_all
            prefix_decay[p] = jnp.broadcast_to(decay_all[:, :HALF], (8, HALF))
            moved = mm_exact_left(near16, jnp.concatenate([near_all, offset_all], axis=1))
            whole = (
                decay * decay_all,
                decay * near_all + decay_all * near + moved[:, :HEAD],
                decay[:, :HALF] * offset_all + moved[:, HEAD:] + offset,
            )
    put_map(mem["sending"], 0, *whole)
    far_slots = mem["far_slots"]

    def far_copy(k):
        return remote(
            "far",
            k,
            mem["sending"].at[0],
            far_slots.at[k],
            {ZAX: lax.rem(z + 2 * k * sign + nz, nz)},
        )

    behind = group + direction * (groups - 1 - 2 * group)
    ahead = groups - 1 - behind
    for k in sorted(range(1, groups), key=lambda k: -min(2 * k, nz - 2 * k)):

        @pl.when(k <= ahead)
        def _(k=k):
            far_copy(k).start()

    for copy in ctx_arriving:
        copy.wait_recv()
    steps = context_steps(
        ctx_all, rate_ref[direction, own_head], bias_ref[direction, own_head],
        direction, own_head, own_half,
    )
    ctx_steps, ctx_decay, state = mem["ctx_steps"], mem["ctx_decay"], mem["state"]
    for b, (step, decay) in enumerate(steps):
        ctx_steps[b] = step
        ctx_decay[b] = jnp.broadcast_to(decay, (8, HALF))
    first = direction * (len(steps) - 1)
    now = ctx_steps[first][:, HEAD:]
    for b in range(1, len(steps)):
        at = first + sign * b
        step = ctx_steps[at]
        now = ctx_decay[at, 0:1, :] * now - mm3(step[:, :HEAD], now) + step[:, HEAD:]
    state[...] = now
    for k in reversed(range(1, groups)):

        @pl.when(k <= behind)
        def _(k=k):
            far_copy(k).wait_recv()
            decay, near16, offset = get_map(far_slots, k)
            now = state[...]
            state[...] = decay[:, :HALF] * now + mm_exact_left(near16, now) + offset

    now = state[...]
    now16 = now.astype(BF16)

    def entering(low, at_x):
        place = low * nx + at_x
        p = place + direction * (members - 1 - 2 * place)
        values = prefix_decay[p, 0:1, :] * now + dot16(prefix_near[p], now16) + prefix_offset[p]
        return pack_halves(values).astype(BF16)

    leaving, states = mem["leaving"], mem["states"]
    mine = low_z * nx + x
    spots = [close_place(dl, dx) for dl, dx in close]
    states[mine] = entering(low_z, x)
    for at, values in zip(close, [entering(low, at_x) for low, at_x in spots]):
        leaving[at[0] * nx + at[1]] = values
    arriving = []
    for (dl, dx), (low, at_x) in zip(close, spots):
        k = dl * nx + dx
        arriving.append(
            begin(
                remote(
                    "back", k, leaving.at[k], states.at[mine], {ZAX: group * 2 + low, XAX: at_x}
                )
            )
        )
    for copy in arriving:
        copy.wait_recv()

    gated, gathered = mem["gated"], mem["gathered"]
    head_gain = loads["out_gain"][...].astype(F32)
    for h in range(HEADS_DEV):
        whole = jnp.concatenate(
            [
                jnp.concatenate(
                    [unpack_halves(states[d * nx + 2 * h + c].astype(F32)) for c in range(2)],
                    axis=1,
                )
                for d in range(2)
            ],
            axis=0,
        ).astype(BF16)
        total = dot16(reads[h], whole) + base[h]
        scaled = total * lax.rsqrt(jnp.mean(total * total, axis=-1, keepdims=True) + norm_eps)
        lanes = slice(h * HEAD, (h + 1) * HEAD)
        result = (scaled * head_gain * mem["gate"][:, lanes]).astype(BF16)
        for t in range(ny):
            gated[t, :, lanes] = result[t * rows_out : (t + 1) * rows_out]
    arriving = []
    for dy in range(1, ny):
        to = lax.rem(y + dy, ny)
        arriving.append(begin(remote("tp", dy, gated.at[to], gathered.at[dy], {YAX: to})))
    fetched["w_out"].wait()
    w_out = loads["w_out"]

    def product(values, owner):
        return dot16(values, w_out[pl.ds(pl.multiple_of(owner * inner, inner), inner), :])

    mixed = product(gated[y], y)
    for dy, copy in zip(range(1, ny), arriving):
        copy.wait_recv()
        mixed = mixed + product(gathered[dy], lax.rem(y - dy + ny, ny))
    own = loads["latent"][0, pl.ds(pl.multiple_of(y * rows_out, 16), rows_out), :].astype(F32)
    out_ref[...] = (own + mod[0:1, 2 * D :] * mixed).astype(BF16)

    for k in range(1, groups):

        @pl.when(k <= ahead)
        def _(k=k):
            far_copy(k).wait_send()

    for copy in started:
        copy.wait_send()


def whole(operands, nz, nx, ny):
    span, ctx_rows = operands["latent"].shape[1], operands["context"].shape[1]
    inner = HEADS_DEV * HEAD
    rows_out = span // ny
    width = operands["w_mod"].shape[1]
    members, groups = 2 * nx, nz // 2
    ctx_blocks = nz * nx * ctx_rows // BLOCK
    memory = {
        "part": ((2, width), F32),
        "mod_slots": ((nz, 2, width), F32),
        "spread": ((nx * ny, 2, width), F32),
        "mod": ((2, width * ny), F32),
        "normed": ((span + ctx_rows, D), F32),
        "rows": ((span + 16, D), BF16),
        "ctx_z": ((HEADS_DEV, nz, ctx_rows, 3 * HEAD), BF16),
        "ctx_all": ((nx, nz, ctx_rows, 3 * HEAD), BF16),
        "maps": ((2 * CHAINS, MAP_ROWS, HEAD), BF16),
        "near_slots": ((members, MAP_ROWS, HEAD), BF16),
        "gate": ((span, inner), F32),
        "reads": ((HEADS_DEV, span, 2 * HEAD), BF16),
        "base": ((HEADS_DEV, span, HEAD), F32),
        "prefix_near": ((members, HEAD, HEAD), BF16),
        "prefix_offset": ((members, HEAD, HALF), F32),
        "prefix_decay": ((members, 8, HALF), F32),
        "sending": ((1, MAP_ROWS, HEAD), BF16),
        "far_slots": ((groups, MAP_ROWS, HEAD), BF16),
        "ctx_steps": ((ctx_blocks, HEAD, HEAD + HALF), F32),
        "ctx_decay": ((ctx_blocks, 8, HALF), F32),
        "state": ((HEAD, HALF), F32),
        "leaving": ((members, HALF, HEAD), BF16),
        "states": ((members, HALF, HEAD), BF16),
        "gated": ((ny, rows_out, inner), BF16),
        "gathered": ((ny, rows_out, inner), BF16),
    }
    counts = {
        "mod1": nz,
        "mod2": nx * ny,
        "ctx": HEADS_DEV * nz,
        "ctx2": nx,
        "near": members,
        "far": groups,
        "back": members,
        "tp": ny,
    }

    def kernel(*refs):
        refs = list(refs)

        def take(names):
            return {name: refs.pop(0) for name in names}

        hbm = take(LOADED)
        out_ref = refs.pop(0)
        loads = take(LOADED)
        load_sem = refs.pop(0)
        mem = take(memory)
        send, recv = take(COMM), take(COMM)
        whole_kernel(
            nz, nx, ny, hbm, out_ref, loads, load_sem, mem, send, recv
        )

    return pl.pallas_call(
        kernel,
        out_shape=jax.ShapeDtypeStruct((rows_out, D), BF16),
        in_specs=[pl.BlockSpec(memory_space=pl.ANY)] * len(LOADED),
        out_specs=pl.BlockSpec(memory_space=pltpu.VMEM),
        scratch_shapes=[
            (pltpu.SMEM if n in IN_SMEM else pltpu.VMEM)(operands[n].shape, operands[n].dtype)
            for n in LOADED
        ]
        + [pltpu.SemaphoreType.DMA((len(LOADED),))]
        + [pltpu.VMEM(*memory[name]) for name in memory]
        + [pltpu.SemaphoreType.DMA((counts[name],)) for name in COMM + COMM],
        compiler_params=pltpu.CompilerParams(collective_id=0, has_side_effects=True),
        name="whole",
    )(*[operands[name] for name in LOADED])


def on_device(
    latent,
    cond,
    context,
    ctx_cond,
    w_mod,
    norm_gain,
    w_query,
    w_key,
    w_value,
    w_outgate,
    w_decay,
    w_beta,
    decay_rate,
    decay_bias,
    extra_decay,
    out_gain,
    w_out,
):
    operands = {
        "cond": cond,
        "ctx_cond": ctx_cond[None, :],
        "w_mod": w_mod,
        "latent": latent,
        "context": context,
        "gain": norm_gain.reshape(D // HEAD, HEAD),
        "w_key": w_key,
        "w_value": w_value,
        "w_decay": jnp.transpose(w_decay, (1, 2, 0)),
        "w_beta": jnp.transpose(w_beta, (1, 2, 0)),
        "extra": extra_decay,
        "w_query": w_query,
        "w_outgate": w_outgate,
        "out_gain": out_gain[None, :],
        "w_out": w_out,
        "rate": decay_rate,
        "bias": decay_bias,
    }
    sizes = [lax.axis_size(name) for name in (ZAX, XAX, YAX)]
    return whole(operands, *sizes)[None]


def solution(mesh):
    torus = Mesh(
        mesh.devices.reshape(-1, 4, mesh.shape["tp"], mesh.shape["dp"]), (ZAX, XAX, YAX, "dp")
    )
    return jax.shard_map(
        on_device,
        mesh=torus,
        in_specs=(
            P("dp", SP, None),
            P("dp", SP),
            P("dp", SP, None),
            P(SP),
            P(SP, "tp"),
            P(),
            P(None, "tp"),
            P(None, "tp"),
            P(None, "tp"),
            P(None, "tp"),
            P(None, None, "tp"),
            P(None, None, "tp"),
            P(None, "tp"),
            P(None, "tp"),
            P("dp", None, "tp", SP),
            P(),
            P(),
        ),
        out_specs=P("dp", SP_TP, None),
        check_vma=False,
    )
```

profile of v0, /device:TPU:2, one launch (start us, length us, event | category | flops | bytes accessed | tf_op | source)
XLA Modules:
  0.0 50.3 jit_solution(7419656502720953902)
XLA Ops:
  0.0 48.7 %whole.1 = bf16[48,2048]{1,0:T(8,128)(2,1)} custom-call(bf16[1,64]{1,0:T(2,128)(2,1)} %refs_0_.1, bf16[1,64]{1,0:T(2,128)(2,1)} %bitcast.10, bf16[64,1536]{1,0:T(8,128)(2,1)} %refs_2_.1, bf16[1,192,2048]{2,1,0:T(8,128)(2,1)} %refs_3_.1, bf16[1,8,2048]{2,1,0:T(8,128)(2,1)} %refs_4_.1, bf16[16,128]{1,0:T(8,128)(2,1)} %bitcast.9, bf16[2048,256]{1,0:T(8,128)(2,1)} %refs_6_.1, ...), custom_call_target="tpu_custom_call" | custom-call | tf_op jit(solution)/shard_map/whole/pallas_call | solution.py:709
  48.7 1.6 %copy.19 = bf16[1,48,2048]{2,1,0:T(8,128)(2,1)} copy(bf16[1,48,2048]{2,1,0:T(8,128)(2,1)} %bitcast.6) | data formatting | bytes 393216
where the time goes:
time: 50.5 us; the launch traced here: 50.3 us
  Pallas kernels  48.7 us (96%)
  local copies, waits for them, and re-layouts  1.62 us (3%)
    pallas_call x1, Pallas kernels, whole(): pl.pallas_call(kernel, out_shape=jax.ShapeDtypeStruct((rows_out, D), BF16...  48.7 us
    unnamed x1, local copies, waits for them, and re-layouts  1.62 us

commit v1 on v0

--- a/solution.py
+++ b/solution.py
@@ -210,7 +210,7 @@
 COMM = ["mod1", "mod2", "ctx", "ctx2", "near", "far", "back", "tp"]
 
 
-def whole_kernel(nz, nx, ny, hbm, out_ref, loads, load_sem, mem, send, recv):
+def whole_kernel(nz, nx, ny, hbm, out_ref, loads, load_sem, mem, send, recv, ready):
     z, x, y = lax.axis_index(ZAX), lax.axis_index(XAX), lax.axis_index(YAX)
     span = loads["latent"].shape[1]
     ctx_rows = loads["context"].shape[1]
@@ -238,10 +238,8 @@
 
     barrier = pltpu.get_barrier_semaphore()
     peers = [{ZAX: lax.rem(z + dz, nz)} for dz in range(1, nz)]
-    peers += [across_target(*at) for at in across]
-    peers += [
-        {ZAX: group * 2 + lax.rem(low_z + 1, 2), XAX: lax.rem(x + dx, nx)} for dx in range(1, nx)
-    ]
+    peers += [{XAX: lax.rem(x + dx, nx)} for dx in range(1, nx)]
+    peers += [{YAX: lax.rem(y + dy, ny)} for dy in range(1, ny)]
     for target in peers:
         pl.semaphore_signal(barrier, inc=1, device_id=target, device_id_type=MESH)
     fetched = {}
@@ -267,6 +265,10 @@
         started.append(copy)
         return copy
 
+    def sends_done():
+        while started:
+            started.pop(0).wait_send()
+
     part, slots, spread = mem["part"], mem["mod_slots"], mem["spread"]
     width = part.shape[1]
     for name in ("cond", "ctx_cond", "w_mod"):
@@ -279,6 +281,16 @@
     arriving = [
         begin(remote("mod1", dz, part, slots.at[dz], {ZAX: lax.rem(z + dz, nz)})) for dz in along
     ]
+    for dx in range(1, nx):
+        pl.semaphore_signal(
+            ready.at[0], inc=1, device_id={XAX: lax.rem(x + dx, nx)}, device_id_type=MESH
+        )
+    pl.semaphore_signal(
+        ready.at[1],
+        inc=1,
+        device_id={ZAX: group * 2 + lax.rem(low_z + 1, 2)},
+        device_id_type=MESH,
+    )
     for name in ("latent", "context", "gain"):
         fetched[name].wait()
     gain = jnp.concatenate(
@@ -298,6 +310,7 @@
         copy.wait_recv()
         summed = summed + slots[dz]
     spread[y * nx + x] = summed
+    pl.semaphore_wait(ready.at[0], nx - 1)
     arriving = [
         begin(
             remote(
@@ -441,6 +454,7 @@
         return ((at_x // 2) * 2 + low) * 2 + lax.rem(at_x, 2)
 
     near_slots[0] = maps[map_index(low_z, x)]
+    pl.semaphore_wait(ready.at[1], 1)
     arriving = []
     for dl, dx in close:
         low, at_x = close_place(dl, dx)
@@ -502,30 +516,27 @@
         mem["prefix_offset"],
         mem["prefix_decay"],
     )
-    whole = None
+    def joined(later, earlier, exact):
+        decay, near, offset = later
+        decay_all, near_all, offset_all = earlier
+        both = jnp.concatenate([near_all, offset_all], axis=1)
+        moved = mm_exact_left(near, both) if exact else mm3(near, both)
+        return (
+            decay * decay_all,
+            decay * near_all + decay_all * near + moved[:, :HEAD],
+            decay[:, :HALF] * offset_all + moved[:, HEAD:] + offset,
+        )
+
+    single = []
     for p in range(members):
         source = p + direction * (members - 1 - 2 * p)
         from_low, from_x = source // nx, lax.rem(source, nx)
         slot = lax.rem(low_z - from_low + 2, 2) * nx + lax.rem(x - from_x + nx, nx)
-        decay, near16, offset = get_map(near_slots, slot)
-        near = near16.astype(F32)
-        if whole is None:
-            prefix_near[0] = jnp.zeros((HEAD, HEAD), BF16)
-            prefix_offset[0] = jnp.zeros((HEAD, HALF), F32)
-            prefix_decay[0] = jnp.ones((8, HALF), F32)
-            whole = (decay, near, offset)
-        else:
-            decay_all, near_all, offset_all = whole
-            prefix_near[p] = near_all.astype(BF16)
-            prefix_offset[p] = offset_all
-            prefix_decay[p] = jnp.broadcast_to(decay_all[:, :HALF], (8, HALF))
-            moved = mm_exact_left(near16, jnp.concatenate([near_all, offset_all], axis=1))
-            whole = (
-                decay * decay_all,
-                decay * near_all + decay_all * near + moved[:, :HEAD],
-                decay[:, :HALF] * offset_all + moved[:, HEAD:] + offset,
-            )
-    put_map(mem["sending"], 0, *whole)
+        decay, near, offset = get_map(near_slots, slot)
+        single.append((decay, near.astype(F32), offset))
+    pairs = [joined(single[p + 1], single[p], True) for p in range(0, members, 2)]
+    fours = [joined(pairs[p + 1], pairs[p], False) for p in range(0, members // 2, 2)]
+    put_map(mem["sending"], 0, *joined(fours[1], fours[0], False))
     far_slots = mem["far_slots"]
 
     def far_copy(k):
@@ -545,6 +556,24 @@
         def _(k=k):
             far_copy(k).start()
 
+    third = joined(pairs[2], fours[0], False)
+    prefixes = [
+        single[0],
+        pairs[0],
+        joined(single[2], pairs[0], True),
+        fours[0],
+        joined(single[4], fours[0], True),
+        third,
+        joined(single[6], third, True),
+    ]
+    prefix_near[0] = jnp.zeros((HEAD, HEAD), BF16)
+    prefix_offset[0] = jnp.zeros((HEAD, HALF), F32)
+    prefix_decay[0] = jnp.ones((8, HALF), F32)
+    for p, (decay, near, offset) in enumerate(prefixes):
+        prefix_near[p + 1] = near.astype(BF16)
+        prefix_offset[p + 1] = offset
+        prefix_decay[p + 1] = jnp.broadcast_to(decay[:, :HALF], (8, HALF))
+    sends_done()
     for copy in ctx_arriving:
         copy.wait_recv()
     steps = context_steps(
@@ -596,6 +625,12 @@
                 )
             )
         )
+    for k in range(1, groups):
+
+        @pl.when(k <= ahead)
+        def _(k=k):
+            far_copy(k).wait_send()
+
     for copy in arriving:
         copy.wait_recv()
 
@@ -629,20 +664,16 @@
         return dot16(values, w_out[pl.ds(pl.multiple_of(owner * inner, inner), inner), :])
 
     mixed = product(gated[y], y)
+    for copy in started[:-(ny - 1)]:
+        copy.wait_send()
+    del started[: -(ny - 1)]
     for dy, copy in zip(range(1, ny), arriving):
         copy.wait_recv()
         mixed = mixed + product(gathered[dy], lax.rem(y - dy + ny, ny))
     own = loads["latent"][0, pl.ds(pl.multiple_of(y * rows_out, 16), rows_out), :].astype(F32)
     out_ref[...] = (own + mod[0:1, 2 * D :] * mixed).astype(BF16)
 
-    for k in range(1, groups):
-
-        @pl.when(k <= ahead)
-        def _(k=k):
-            far_copy(k).wait_send()
-
-    for copy in started:
-        copy.wait_send()
+    sends_done()
 
 
 def whole(operands, nz, nx, ny):
@@ -703,7 +734,7 @@
         mem = take(memory)
         send, recv = take(COMM), take(COMM)
         whole_kernel(
-            nz, nx, ny, hbm, out_ref, loads, load_sem, mem, send, recv
+            nz, nx, ny, hbm, out_ref, loads, load_sem, mem, send, recv, refs.pop(0)
         )
 
     return pl.pallas_call(
@@ -717,7 +748,8 @@
         ]
         + [pltpu.SemaphoreType.DMA((len(LOADED),))]
         + [pltpu.VMEM(*memory[name]) for name in memory]
-        + [pltpu.SemaphoreType.DMA((counts[name],)) for name in COMM + COMM],
+        + [pltpu.SemaphoreType.DMA((counts[name],)) for name in COMM + COMM]
+        + [pltpu.SemaphoreType.REGULAR((2,))],
         compiler_params=pltpu.CompilerParams(collective_id=0, has_side_effects=True),
         name="whole",
     )(*[operands[name] for name in LOADED])

time: 50.5 us -> 49.7 us (0.984)
  Pallas kernels: 48.7 us -> 48 us
    pallas_call x1, Pallas kernels: 48.7 us -> 48 us  [whole(): pl.pallas_call(kernel, out_shape=jax.ShapeDtypeStruct((rows_out, D), BF16...]
where the time goes in v1:
time: 49.7 us; the launch traced here: 49.6 us
  Pallas kernels  48 us (97%)
  local copies, waits for them, and re-layouts  1.62 us (3%)
    pallas_call x1, Pallas kernels, whole(): pl.pallas_call(kernel, out_shape=jax.ShapeDtypeStruct((rows_out, D), BF16...  48 us
    unnamed x1, local copies, waits for them, and re-layouts  1.62 us

profile of v1, /device:TPU:2, one launch (start us, length us, event | category | flops | bytes accessed | tf_op | source)
XLA Modules:
  0.0 49.6 jit_solution(8967939186098328698)
XLA Ops:
  0.0 48.0 %whole.1 = bf16[48,2048]{1,0:T(8,128)(2,1)} custom-call(bf16[1,64]{1,0:T(2,128)(2,1)} %refs_0_.1, bf16[1,64]{1,0:T(2,128)(2,1)} %bitcast.10, bf16[64,1536]{1,0:T(8,128)(2,1)} %refs_2_.1, bf16[1,192,2048]{2,1,0:T(8,128)(2,1)} %refs_3_.1, bf16[1,8,2048]{2,1,0:T(8,128)(2,1)} %refs_4_.1, bf16[16,128]{1,0:T(8,128)(2,1)} %bitcast.9, bf16[2048,256]{1,0:T(8,128)(2,1)} %refs_6_.1, ...), custom_call_target="tpu_custom_call" | custom-call | tf_op jit(solution)/shard_map/whole/pallas_call | solution.py:740
  48.0 1.6 %copy.19 = bf16[1,48,2048]{2,1,0:T(8,128)(2,1)} copy(bf16[1,48,2048]{2,1,0:T(8,128)(2,1)} %bitcast.6) | data formatting | bytes 393216

commit v2 on v1

--- a/solution.py
+++ b/solution.py
@@ -91,10 +91,10 @@
     results = [eye - coupling(low, place, 0) for low, place in zip(lows, places)]
     for level in range(1, (BLOCK - 1).bit_length()):
         inner = [
-            mm3(coupling(low, place, level), result)
+            mm1(coupling(low, place, level), result)
             for low, place, result in zip(lows, places, results)
         ]
-        results = [result - mm3(result, term) for result, term in zip(results, inner)]
+        results = [result - mm1(result, term) for result, term in zip(results, inner)]
     return results
 
 
@@ -183,7 +183,7 @@
         jobs.append((right, decayed, final))
     steps = []
     for (right, decayed, final), inverse in zip(jobs, unit_inverses(lows, [place] * len(lows))):
-        steps.append((mm1(decayed, mm3(inverse, right), TN), jnp.exp(final)))
+        steps.append((mm1(decayed, mm1(inverse, right), TN), jnp.exp(final)))
     return steps
 
 
@@ -422,7 +422,7 @@
     inverses = unit_inverses(lows, orders)
     found = {}
     for (h, d, b, right, decayed, weights, grown, final), inverse in zip(jobs, inverses):
-        solved = mm3(inverse, right)
+        solved = mm1(inverse, right)
         step = mm1(decayed, solved, TN)
         found[h, d, b] = (-step[:, :HEAD], step[:, HEAD:], jnp.exp(final), solved, weights, grown)
     maps = mem["maps"]
@@ -739,7 +739,7 @@
 
     return pl.pallas_call(
         kernel,
-        out_shape=jax.ShapeDtypeStruct((rows_out, D), BF16),
+        out_shape=pltpu.VMEM((rows_out, D), BF16),
         in_specs=[pl.BlockSpec(memory_space=pl.ANY)] * len(LOADED),
         out_specs=pl.BlockSpec(memory_space=pltpu.VMEM),
         scratch_shapes=[

time: 49.7 us -> 46.4 us (0.934)
  Pallas kernels: 48 us -> 45.7 us
  local copies, waits for them, and re-layouts: 1.62 us -> 0.68 us
    pallas_call x1, Pallas kernels: 48 us -> 45.7 us  [whole(): pl.pallas_call(kernel, out_shape=pltpu.VMEM((rows_out, D), BF16), in_spec...]
    unnamed x1, local copies, waits for them, and re-layouts: 1.62 us -> 0.68 us
where the time goes in v2:
time: 46.4 us; the launch traced here: 46.3 us
  Pallas kernels  45.7 us (98%)
  local copies, waits for them, and re-layouts  0.68 us (1%)
    pallas_call x1, Pallas kernels, whole(): pl.pallas_call(kernel, out_shape=pltpu.VMEM((rows_out, D), BF16), in_spec...  45.7 us

profile of v2, /device:TPU:2, one launch (start us, length us, event | category | flops | bytes accessed | tf_op | source)
XLA Modules:
  0.0 46.3 jit_solution(13371599525625737178)
XLA Ops:
  0.0 45.7 %whole.1 = bf16[48,2048]{1,0:T(8,128)(2,1)S(1)} custom-call(bf16[1,64]{1,0:T(2,128)(2,1)} %refs_0_.1, bf16[1,64]{1,0:T(2,128)(2,1)} %bitcast.10, bf16[64,1536]{1,0:T(8,128)(2,1)} %refs_2_.1, bf16[1,192,2048]{2,1,0:T(8,128)(2,1)} %refs_3_.1, bf16[1,8,2048]{2,1,0:T(8,128)(2,1)} %refs_4_.1, bf16[16,128]{1,0:T(8,128)(2,1)} %bitcast.9, ...), custom_call_target="tpu_custom_call" | custom-call | tf_op jit(solution)/shard_map/whole/pallas_call | solution.py:740
  45.7 0.7 %copy.19 = bf16[1,48,2048]{2,1,0:T(8,128)(2,1)} copy(bf16[1,48,2048]{2,1,0:T(8,128)(2,1)S(1)} %bitcast.6) | data formatting | bytes 393216

commit v3 on v2

--- a/solution.py
+++ b/solution.py
@@ -43,24 +43,10 @@
     return high, (values - high.astype(F32)).astype(BF16)
 
 
-def mm3(left, right, dims=NN):
-    left_high, left_low = halves(left)
-    right_high, right_low = halves(right)
-    return dot16(left_high, right_high, dims) + (
-        dot16(left_high, right_low, dims) + dot16(left_low, right_high, dims)
-    )
-
-
 def mm_exact_left(left, right, dims=NN):
     high, low = halves(right)
     left = left.astype(BF16)
     return dot16(left, high, dims) + dot16(left, low, dims)
-
-
-def mm_full(left, right, dims=NN):
-    return lax.dot_general(
-        left, right, dims, preferred_element_type=F32, precision=lax.Precision.HIGHEST
-    )
 
 
 def silu(values):
@@ -172,10 +158,10 @@
     jobs, lows = [], []
     for b in range(tokens // BLOCK):
         part = slice(b * BLOCK, (b + 1) * BLOCK)
-        sums = mm_full(tri, jnp.broadcast_to(log_decay[part], (BLOCK, HEAD)))[:, :1]
+        sums = mm_exact_left(tri, jnp.broadcast_to(log_decay[part], (BLOCK, HEAD)))[:, :1]
         final = jnp.sum(log_decay[part], axis=0, keepdims=True)
         keys, values = keys_all[part], values_all[part]
-        gram = mm3(keys, keys, NT)
+        gram = mm1(keys, keys, NT)
         low, right, decayed, _, _ = chain_terms(
             keys, values, gram, sums, final, betas[part], place
         )
@@ -330,7 +316,7 @@
     ).astype(BF16)
     extra = jnp.concatenate([loads["extra"][0, d] for d in range(2)], axis=0)
     eye_span = (iota2((span, span), 0) == iota2((span, span), 1)).astype(F32)
-    added = mm_full(eye_span, extra, NT)
+    added = mm_exact_left(eye_span, extra, NT)
     for copy in arriving:
         copy.wait_recv()
     mod = mem["mod"]
@@ -396,7 +382,10 @@
     places = [(row, col), (BLOCK - 1 - row, BLOCK - 1 - col)]
     tris = [(row >= col).astype(F32), (row <= col).astype(F32)]
     sums = [
-        [mm_full(tris[d], log_decay[b * BLOCK : (b + 1) * BLOCK]) for b in range(blocks)]
+        [
+            mm_exact_left(tris[d], log_decay[b * BLOCK : (b + 1) * BLOCK])
+            for b in range(blocks)
+        ]
         for d in range(2)
     ]
     jobs, lows, orders, key_parts = [], [], [], {}
@@ -408,7 +397,7 @@
             at = slice(b * BLOCK, (b + 1) * BLOCK)
             keys, values = keys_h[at], values_h[at]
             key_parts[h, b] = keys
-            gram = mm3(keys, keys, NT)
+            gram = mm1(keys, keys, NT)
             for d in range(2):
                 lane = d * HEADS_DEV + h
                 cums = sums[d][b][:, lane : lane + 1]
@@ -516,11 +505,11 @@
         mem["prefix_offset"],
         mem["prefix_decay"],
     )
-    def joined(later, earlier, exact):
+    def joined(later, earlier):
         decay, near, offset = later
         decay_all, near_all, offset_all = earlier
         both = jnp.concatenate([near_all, offset_all], axis=1)
-        moved = mm_exact_left(near, both) if exact else mm3(near, both)
+        moved = mm1(near, both)
         return (
             decay * decay_all,
             decay * near_all + decay_all * near + moved[:, :HEAD],
@@ -534,9 +523,9 @@
         slot = lax.rem(low_z - from_low + 2, 2) * nx + lax.rem(x - from_x + nx, nx)
         decay, near, offset = get_map(near_slots, slot)
         single.append((decay, near.astype(F32), offset))
-    pairs = [joined(single[p + 1], single[p], True) for p in range(0, members, 2)]
-    fours = [joined(pairs[p + 1], pairs[p], False) for p in range(0, members // 2, 2)]
-    put_map(mem["sending"], 0, *joined(fours[1], fours[0], False))
+    pairs = [joined(single[p + 1], single[p]) for p in range(0, members, 2)]
+    fours = [joined(pairs[p + 1], pairs[p]) for p in range(0, members // 2, 2)]
+    put_map(mem["sending"], 0, *joined(fours[1], fours[0]))
     far_slots = mem["far_slots"]
 
     def far_copy(k):
@@ -556,15 +545,15 @@
         def _(k=k):
             far_copy(k).start()
 
-    third = joined(pairs[2], fours[0], False)
+    third = joined(pairs[2], fours[0])
     prefixes = [
         single[0],
         pairs[0],
-        joined(single[2], pairs[0], True),
+        joined(single[2], pairs[0]),
         fours[0],
-        joined(single[4], fours[0], True),
+        joined(single[4], fours[0]),
         third,
-        joined(single[6], third, True),
+        joined(single[6], third),
     ]
     prefix_near[0] = jnp.zeros((HEAD, HEAD), BF16)
     prefix_offset[0] = jnp.zeros((HEAD, HALF), F32)
@@ -589,7 +578,7 @@
     for b in range(1, len(steps)):
         at = first + sign * b
         step = ctx_steps[at]
-        now = ctx_decay[at, 0:1, :] * now - mm3(step[:, :HEAD], now) + step[:, HEAD:]
+        now = ctx_decay[at, 0:1, :] * now - mm1(step[:, :HEAD], now) + step[:, HEAD:]
     state[...] = now
     for k in reversed(range(1, groups)):
 
@@ -598,7 +587,7 @@
             far_copy(k).wait_recv()
             decay, near16, offset = get_map(far_slots, k)
             now = state[...]
-            state[...] = decay[:, :HALF] * now + mm_exact_left(near16, now) + offset
+            state[...] = decay[:, :HALF] * now + mm1(near16, now) + offset
 
     now = state[...]
     now16 = now.astype(BF16)

time: 46.4 us -> 45.8 us (0.987)
  Pallas kernels: 45.7 us -> 45.1 us
    pallas_call x1, Pallas kernels: 45.7 us -> 45.1 us  [whole(): pl.pallas_call(kernel, out_shape=pltpu.VMEM((rows_out, D), BF16), in_spec...]
where the time goes in v3:
time: 45.8 us
  Pallas kernels  45.1 us (98%)
  local copies, waits for them, and re-layouts  0.68 us (1%)
    pallas_call x1, Pallas kernels, whole(): pl.pallas_call(kernel, out_shape=pltpu.VMEM((rows_out, D), BF16), in_spec...  45.1 us

profile of v3, /device:TPU:2, one launch (start us, length us, event | category | flops | bytes accessed | tf_op | source)
XLA Modules:
  0.0 45.8 jit_solution(5832810503786946338)
XLA Ops:
  0.0 45.1 %whole.1 = bf16[48,2048]{1,0:T(8,128)(2,1)S(1)} custom-call(bf16[1,64]{1,0:T(2,128)(2,1)} %refs_0_.1, bf16[1,64]{1,0:T(2,128)(2,1)} %bitcast.10, bf16[64,1536]{1,0:T(8,128)(2,1)} %refs_2_.1, bf16[1,192,2048]{2,1,0:T(8,128)(2,1)} %refs_3_.1, bf16[1,8,2048]{2,1,0:T(8,128)(2,1)} %refs_4_.1, bf16[16,128]{1,0:T(8,128)(2,1)} %bitcast.9, ...), custom_call_target="tpu_custom_call" | custom-call | tf_op jit(solution)/shard_map/whole/pallas_call | solution.py:729
  45.1 0.7 %copy.19 = bf16[1,48,2048]{2,1,0:T(8,128)(2,1)} copy(bf16[1,48,2048]{2,1,0:T(8,128)(2,1)S(1)} %bitcast.6) | data formatting | bytes 393216
